TPU v7x, 32 devices: a whole 2x2x4 slice. The times are simulated.
32 devices in a mesh: dp: 4 (over y, x), kv: 4 (over z), tp: 2 (over core).
Axes of the slice: x: 2, y: 2, z: 4, core: 2. Of those that a mesh axis runs over, the one named last changes fastest.
Arguments:
- tokens: bfloat16 [32, 4096], P('dp', ('kv', 'tp')), may hold values from -6 to 6
- w_query: bfloat16 [4096, 2, 1024], P(None, 'tp', 'kv'), may hold values from -0.09375 to 0.09375
- w_forget: bfloat16 [4096, 2, 1024], P(None, 'tp', 'kv'), may hold values from -0.09375 to 0.09375
- w_input: bfloat16 [4096, 2, 1024], P(None, 'tp', 'kv'), may hold values from -0.09375 to 0.09375
- w_output_gate: bfloat16 [4096, 2, 1024], P(None, 'tp', 'kv'), may hold values from -0.09375 to 0.09375
- gate_floor: float32 [2048], P('tp'), may hold values from 0 to 0.9
- head_gain: float32 [128], replicated, may hold values from 0.1 to 1.9
- w_out: bfloat16 [2048, 4096], P(None, ('kv', 'tp')), may hold values from -0.125 to 0.125
- mix_gain: float32 [4096], replicated, may hold values from 0.1 to 1.9
- ffn_gain: float32 [4096], replicated, may hold values from 0.1 to 1.9
- w_up: bfloat16 [4096, 16384], P(None, ('kv', 'tp')), may hold values from -0.09375 to 0.09375
- w_down: bfloat16 [16384, 4096], P(('kv', 'tp')), may hold values from -0.0625 to 0.0625
- state: float32 [32, 16, 128, 128], P(('dp', 'kv'), 'tp'), may hold values from -6 to 6
Outputs:
- mixed: bfloat16 [32, 4096], P('dp', ('kv', 'tp'))
- new_state: float32 [32, 16, 128, 128], P(('dp', 'kv'), 'tp')
All inputs are finite; a program needn't handle non-finite values.
Results may differ from a plain program's by a relative error of at most 0.014.
Values may be sent and summed in bfloat16 or wider, within the bound.
A program may use at most 128 MiB of HBM per device.

v0:
```python
import jax
import jax.numpy as jnp
from jax import lax
from jax.sharding import PartitionSpec as P

EPSILON = 1e-06


def rms_scale(values, gain):
    return values * lax.rsqrt(jnp.mean(values * values, axis=-1, keepdims=True) + EPSILON) * gain


def per_device(
    tokens,
    w_query,
    w_forget,
    w_input,
    w_output_gate,
    gate_floor,
    head_gain,
    w_out,
    mix_gain,
    ffn_gain,
    w_up,
    w_down,
    state,
):
    group_kv = lax.axis_size("kv")
    group_tp = lax.axis_size("tp")
    tokens_f = tokens.astype(jnp.float32)
    full_rows = lax.all_gather(tokens, ("kv", "tp"), axis=1, tiled=True)
    normed = rms_scale(full_rows.astype(jnp.float32), mix_gain).astype(jnp.bfloat16)

    def project(weight):
        return jnp.dot(normed, weight[:, 0, :], preferred_element_type=jnp.float32).astype(
            jnp.bfloat16
        )

    query_raw, forget_raw, input_raw, gate_raw = (
        lax.all_to_all(project(w_query), "kv", split_axis=0, concat_axis=1, tiled=True),
        lax.all_to_all(project(w_forget), "kv", split_axis=0, concat_axis=1, tiled=True),
        lax.all_to_all(project(w_input), "kv", split_axis=0, concat_axis=1, tiled=True),
        lax.all_to_all(project(w_output_gate), "kv", split_axis=0, concat_axis=1, tiled=True),
    )
    seq_local = state.shape[0]
    heads_local = state.shape[1]
    head_size = state.shape[2]
    query_vec = query_raw.astype(jnp.float32).reshape(
        seq_local, heads_local, head_size
    ) * head_size ** (-0.5)
    floor_heads = gate_floor.reshape(heads_local, head_size)
    forget_gate = floor_heads + (1.0 - floor_heads) * jax.nn.sigmoid(
        forget_raw.astype(jnp.float32).reshape(seq_local, heads_local, head_size)
    )
    input_vec = input_raw.astype(jnp.float32).reshape(seq_local, heads_local, head_size)
    gate_vec = gate_raw.astype(jnp.float32).reshape(seq_local, heads_local, head_size)
    new_state = (
        forget_gate[..., None] * state + (1.0 - forget_gate)[..., None] * input_vec[:, :, None, :]
    )
    head_out = jnp.einsum("bhk,bhkv->bhv", query_vec, new_state, precision=lax.Precision.HIGHEST)
    branch = rms_scale(head_out, head_gain) * jax.nn.silu(gate_vec)
    branch = branch.reshape(seq_local, 1, heads_local * head_size).astype(jnp.bfloat16)
    gathered = lax.all_gather(branch, ("kv", "tp"), axis=1, tiled=True)
    gathered = gathered.reshape(seq_local, group_kv, group_tp, heads_local * head_size)
    gathered = jnp.transpose(gathered, (1, 0, 2, 3)).reshape(
        group_kv * seq_local, group_tp * heads_local * head_size
    )
    projected = jnp.dot(gathered, w_out, preferred_element_type=jnp.float32)
    residual_one = (tokens_f + projected).astype(jnp.bfloat16)
    whole_rows = lax.all_gather(residual_one, ("kv", "tp"), axis=1, tiled=True)
    ffn_in = rms_scale(whole_rows.astype(jnp.float32), ffn_gain).astype(jnp.bfloat16)
    upward = jnp.dot(ffn_in, w_up, preferred_element_type=jnp.float32)
    hidden = jnp.square(jax.nn.relu(upward)).astype(jnp.bfloat16)
    partial_terms = jnp.dot(hidden, w_down, preferred_element_type=jnp.float32)
    summed = lax.psum_scatter(partial_terms, ("kv", "tp"), scatter_dimension=1, tiled=True)
    results = (residual_one.astype(jnp.float32) + summed).astype(jnp.bfloat16)
    return (results, new_state)


def solution(mesh):
    placed = (
        P("dp", ("kv", "tp")),
        P(None, "tp", "kv"),
        P(None, "tp", "kv"),
        P(None, "tp", "kv"),
        P(None, "tp", "kv"),
        P("tp"),
        P(),
        P(None, ("kv", "tp")),
        P(),
        P(),
        P(None, ("kv", "tp")),
        P(("kv", "tp"), None),
        P(("dp", "kv"), "tp", None, None),
    )
    return jax.shard_map(
        per_device,
        mesh=mesh,
        in_specs=placed,
        out_specs=(P("dp", ("kv", "tp")), P(("dp", "kv"), "tp", None, None)),
        check_vma=False,
    )
```

profile of v0, /device:TPU:0, one launch (start us, length us, event | category | flops | bytes accessed | tf_op | source)
XLA Modules:
  0.0 146.4 jit_solution(5957048308820464604)
XLA Ops:
  7.2 0.0 copy-start
  7.2 0.0 copy-start.4
  7.2 16.0 %all_gather.9 = bf16[8,4096]{1,0:T(8,128)(2,1)S(1)} all-gather(bf16[8,512]{1,0:T(8,128)(2,1)} %param.13), channel_id=1, replica_groups=mesh['dp'=4,'kv'=4,'tp'=2] {'kv','tp'}, dimensions={1}, use_global_device_ids=true | all-gather | bytes 73728 | tf_op jit(solution)/shard_map/all_gather | solution.py:31
  23.2 0.1 fusion.24
  23.4 2.0 %fusion.20 = bf16[8,256]{1,0:T(8,128)(2,1)S(1)} fusion(bf16[4096,1,256]{2,0,1:T(8,128)(2,1)} %param.17, bf16[8,4096]{1,0:T(8,128)(2,1)S(1)} %all_gather.9, f32[4096]{0:T(1024)} %param.21, f32[8]{0:T(128)S(1)} %add_rsqrt_fusion.2), kind=kOutput, calls=%fused_computation.16 | convolution fusion | flops 16910336 | bytes 2183200 | tf_op jit(solution)/shard_map/dot_general | solution.py:35
  25.4 0.6 all_to_all.46
  26.0 4.6 %all-to-all-start.3 = ((bf16[4,2,256]{2,1,0:T(2,128)(2,1)}), bf16[4,2,256]{2,1,0:T(2,128)(2,1)S(1)}, u32[]{:S(2)}, u32[]{:S(2)}) async-start(bf16[4,2,256]{2,1,0:T(2,128)(2,1)} %all_to_all.46), calls=%async_computation.3 | async-start | bytes 8192 | tf_op jit(solution)/shard_map/all_to_all | solution.py:43
  30.7 0.0 copy-done.4
  30.7 0.0 copy-start.2
  30.7 0.0 copy-start.3
  30.7 2.2 %fusion.14 = bf16[8,256]{1,0:T(8,128)(2,1)S(1)} fusion(bf16[4096,1,256]{2,0,1:T(8,128)(2,1)} %param.15, bf16[8,4096]{1,0:T(8,128)(2,1)S(1)} %all_gather.9, f32[4096]{0:T(1024)S(1)} %copy-done.4, f32[8]{0:T(128)S(1)} %add_rsqrt_fusion.2), kind=kOutput, calls=%fused_computation.14 | convolution fusion | flops 16910336 | bytes 2183200 | tf_op jit(solution)/shard_map/dot_general | solution.py:35
  32.8 0.1 copy-done.2
  32.9 0.0 copy-start.7
  32.9 0.4 fusion.17
  33.3 0.2 copy-done.3
  33.5 0.4 fusion.11
  33.9 0.0 copy-done.7
  33.9 0.0 copy-start.8
  33.9 0.0 copy-start.5
  34.0 0.6 all_to_all.42
  34.6 0.6 all_to_all.44
  35.2 0.6 all_to_all.40
  35.8 0.5 all-to-all-done.3
  36.2 4.6 %all-to-all-start = ((bf16[4,2,256]{2,1,0:T(2,128)(2,1)}), bf16[4,2,256]{2,1,0:T(2,128)(2,1)S(1)}, u32[]{:S(2)}, u32[]{:S(2)}) async-start(bf16[4,2,256]{2,1,0:T(2,128)(2,1)} %all_to_all.40), calls=%async_computation | async-start | bytes 8192 | tf_op jit(solution)/shard_map/all_to_all | solution.py:40
  40.9 5.6 %all-to-all-done = bf16[4,2,256]{2,1,0:T(2,128)(2,1)S(1)} async-done(((bf16[4,2,256]{2,1,0:T(2,128)(2,1)}), bf16[4,2,256]{2,1,0:T(2,128)(2,1)S(1)}, u32[]{:S(2)}, u32[]{:S(2)}) %all-to-all-start) | async-done | bytes 4128 | tf_op jit(solution)/shard_map/all_to_all | solution.py:40
  46.4 3.2 %all-to-all-start.2 = ((bf16[4,2,256]{2,1,0:T(2,128)(2,1)}), bf16[4,2,256]{2,1,0:T(2,128)(2,1)S(1)}, u32[]{:S(2)}, u32[]{:S(2)}) async-start(bf16[4,2,256]{2,1,0:T(2,128)(2,1)} %all_to_all.44), calls=%async_computation.2 | async-start | bytes 8192 | tf_op jit(solution)/shard_map/all_to_all | solution.py:42
  49.7 5.5 %all-to-all-done.2 = bf16[4,2,256]{2,1,0:T(2,128)(2,1)S(1)} async-done(((bf16[4,2,256]{2,1,0:T(2,128)(2,1)}), bf16[4,2,256]{2,1,0:T(2,128)(2,1)S(1)}, u32[]{:S(2)}, u32[]{:S(2)}) %all-to-all-start.2) | async-done | bytes 4128 | tf_op jit(solution)/shard_map/all_to_all | solution.py:42
  55.2 3.2 %all-to-all-start.1 = ((bf16[4,2,256]{2,1,0:T(2,128)(2,1)}), bf16[4,2,256]{2,1,0:T(2,128)(2,1)S(1)}, u32[]{:S(2)}, u32[]{:S(2)}) async-start(bf16[4,2,256]{2,1,0:T(2,128)(2,1)} %all_to_all.42), calls=%async_computation.1 | async-start | bytes 8192 | tf_op jit(solution)/shard_map/all_to_all | solution.py:41
  58.4 0.0 reduce-scatter.2.cloned.1.call-start
  58.6 5.4 %all-to-all-done.1 = bf16[4,2,256]{2,1,0:T(2,128)(2,1)S(1)} async-done(((bf16[4,2,256]{2,1,0:T(2,128)(2,1)}), bf16[4,2,256]{2,1,0:T(2,128)(2,1)S(1)}, u32[]{:S(2)}, u32[]{:S(2)}) %all-to-all-start.1) | async-done | bytes 4128 | tf_op jit(solution)/shard_map/all_to_all | solution.py:41
  64.0 1.8 %multiply_add_fusion = f32[2,8,128,128]{3,2,1,0:T(8,128)S(1)} fusion(f32[2,8,128,128]{3,2,1,0:T(8,128)} %param.25, f32[2,8,128]{2,1,0:T(8,128)S(1)} %reshape.112, f32[2,8,128]{2,1,0:T(8,128)S(1)} %get-tuple-element.2, f32[2,8,128]{2,1,0:T(8,128)S(1)} %get-tuple-element.3), kind=kLoop, calls=%fused_computation.17 | loop fusion | flops 786432 | bytes 2121728 | tf_op jit(solution)/shard_map/add | solution.py:58
  65.9 0.0 copy-start.1
  65.9 0.0 copy-start.6
  65.9 1.0 fusion.42
  66.9 0.1 multiply_reduce_fusion
  67.0 0.0 copy-done.8
  67.0 0.1 multiply_convert_fusion
  67.1 14.1 %all_gather.10 = bf16[2,8,1024]{2,0,1:T(2,128)(2,1)S(1)} all-gather(bf16[2,1,1024]{2,0,1:T(2,128)(2,1)S(1)} %convert_element_type.111), channel_id=1, replica_groups=mesh['dp'=4,'kv'=4,'tp'=2] {'kv','tp'}, dimensions={1}, use_global_device_ids=true | all-gather | bytes 36864 | tf_op jit(solution)/shard_map/all_gather | solution.py:63
  81.2 0.0 copy-done
  81.2 0.0 copy-done.5
  81.2 0.4 fusion.10
  81.6 14.0 %all_gather.11 = bf16[8,4096]{1,0:T(8,128)(2,1)S(1)} all-gather(bf16[8,512]{1,0:T(8,128)(2,1)S(1)} %fusion.10), channel_id=1, replica_groups=mesh['dp'=4,'kv'=4,'tp'=2] {'kv','tp'}, dimensions={1}, use_global_device_ids=true | all-gather | bytes 73728 | tf_op jit(solution)/shard_map/all_gather | solution.py:70
  95.6 0.1 fusion.27
  95.7 0.0 copy-done.6
  95.7 13.5 %fusion.23 = f32[8,4096]{1,0:T(8,128)} fusion(bf16[2048,4096]{1,0:T(8,128)(2,1)} %param.24, bf16[4096,2048]{1,0:T(8,128)(2,1)} %param.23, bf16[8,4096]{1,0:T(8,128)(2,1)S(1)} %all_gather.11, f32[4096]{0:T(1024)S(1)} %copy-done.6, f32[8]{0:T(128)S(1)} %add_rsqrt_fusion.1), kind=kOutput, calls=%fused_computation.18 | convolution fusion | flops 268615680 | bytes 33767456 | tf_op jit(solution)/shard_map/dot_general | solution.py:74
  109.3 0.0 copy-done.1
  109.3 0.0 reduce-scatter.2.cloned.1.call-update
  109.3 28.9 %reduce-scatter.2.cloned.1.call-done = f32[8,512]{1,0:T(8,128)} async-done(((f32[8,4096]{1,0:T(8,128)}), f32[8,512]{1,0:T(8,128)}) %reduce-scatter.2.cloned.1.call-update) | async-done | bytes 16400 | tf_op jit(solution)/shard_map/reduce_scatter | solution.py:75
  138.2 1.3 add_convert_fusion
  (20 shorter events, 0.2 us)
Async XLA Ops:
  7.2 74.0 %copy-start = (bf16[2048,512]{1,0:T(8,128)(2,1)S(1)}, bf16[2048,512]{1,0:T(8,128)(2,1)}, u32[]{:S(2)}) copy-start(bf16[2048,512]{1,0:T(8,128)(2,1)} %param.20) | copy-start | bytes 6291460
  7.2 23.5 %copy-start.4 = (f32[4096]{0:T(1024)S(1)}, f32[4096]{0:T(1024)}, u32[]{:S(2)}) copy-start(f32[4096]{0:T(1024)} %param.21) | copy-start | bytes 49156
  26.0 10.2 %all-to-all-start.3 = ((bf16[4,2,256]{2,1,0:T(2,128)(2,1)}), bf16[4,2,256]{2,1,0:T(2,128)(2,1)S(1)}, u32[]{:S(2)}, u32[]{:S(2)}) async-start(bf16[4,2,256]{2,1,0:T(2,128)(2,1)} %all_to_all.46), calls=%async_computation.3 | async-start | bytes 8192 | tf_op jit(solution)/shard_map/all_to_all | solution.py:43
  30.7 2.2 %copy-start.2 = (bf16[4096,1,256]{2,0,1:T(8,128)(2,1)S(1)}, bf16[4096,1,256]{2,0,1:T(8,128)(2,1)}, u32[]{:S(2)}) copy-start(bf16[4096,1,256]{2,0,1:T(8,128)(2,1)} %param.16) | copy-start | bytes 6291460
  30.7 2.9 %copy-start.3 = (bf16[4096,1,256]{2,0,1:T(8,128)(2,1)S(1)}, bf16[4096,1,256]{2,0,1:T(8,128)(2,1)}, u32[]{:S(2)}) copy-start(bf16[4096,1,256]{2,0,1:T(8,128)(2,1)} %param.14) | copy-start | bytes 6291460
  32.9 1.0 copy-start.7
  33.9 33.0 %copy-start.8 = (f32[128]{0:T(128)S(1)}, f32[128]{0:T(128)}, u32[]{:S(2)}) copy-start(f32[128]{0:T(128)} %param.19) | copy-start | bytes 1540
  33.9 47.3 %copy-start.5 = (bf16[8,512]{1,0:T(8,128)(2,1)S(1)}, bf16[8,512]{1,0:T(8,128)(2,1)}, u32[]{:S(2)}) copy-start(bf16[8,512]{1,0:T(8,128)(2,1)} %param.13) | copy-start | bytes 24580
  36.2 10.2 %all-to-all-start = ((bf16[4,2,256]{2,1,0:T(2,128)(2,1)}), bf16[4,2,256]{2,1,0:T(2,128)(2,1)S(1)}, u32[]{:S(2)}, u32[]{:S(2)}) async-start(bf16[4,2,256]{2,1,0:T(2,128)(2,1)} %all_to_all.40), calls=%async_computation | async-start | bytes 8192 | tf_op jit(solution)/shard_map/all_to_all | solution.py:40
  46.4 8.8 %all-to-all-start.2 = ((bf16[4,2,256]{2,1,0:T(2,128)(2,1)}), bf16[4,2,256]{2,1,0:T(2,128)(2,1)S(1)}, u32[]{:S(2)}, u32[]{:S(2)}) async-start(bf16[4,2,256]{2,1,0:T(2,128)(2,1)} %all_to_all.44), calls=%async_computation.2 | async-start | bytes 8192 | tf_op jit(solution)/shard_map/all_to_all | solution.py:42
  55.2 8.8 %all-to-all-start.1 = ((bf16[4,2,256]{2,1,0:T(2,128)(2,1)}), bf16[4,2,256]{2,1,0:T(2,128)(2,1)S(1)}, u32[]{:S(2)}, u32[]{:S(2)}) async-start(bf16[4,2,256]{2,1,0:T(2,128)(2,1)} %all_to_all.42), calls=%async_computation.1 | async-start | bytes 8192 | tf_op jit(solution)/shard_map/all_to_all | solution.py:41
  58.4 79.8 %reduce-scatter.2.cloned.1.call-start = ((), (), s32[]{:S(2)}) async-start(), calls=%async_computation.5 | async-start | bytes 147456 | tf_op jit(solution)/shard_map/reduce_scatter | solution.py:75
  65.9 43.4 %copy-start.1 = (f32[2,8,128,128]{3,2,1,0:T(8,128)}, f32[2,8,128,128]{3,2,1,0:T(8,128)S(1)}, u32[]{:S(2)}) copy-start(f32[2,8,128,128]{3,2,1,0:T(8,128)S(1)} %multiply_add_fusion) | copy-start | bytes 3145732
  65.9 29.9 %copy-start.6 = (f32[4096]{0:T(1024)S(1)}, f32[4096]{0:T(1024)}, u32[]{:S(2)}) copy-start(f32[4096]{0:T(1024)} %param.22) | copy-start | bytes 49156
Sparse Core Ops, SparseCore 0:
  109.4 28.7 reduce-scatter.1
where the time goes:
time: 147 us; the launch traced here: 146 us
  waiting for transfers between devices  45.9 us (31%)
  blocking collectives  44.1 us (30%)
  matrix products  19.9 us (14%)
  starting transfers between devices  15.7 us (11%)
  between operations  14.2 us (10%)
  other arithmetic  3.68 us (3%)
  local copies, waits for them, and re-layouts  2.83 us (2%)
    reduce_scatter x1, waiting for transfers between devices, per_device(): lax.psum_scatter(partial_terms, ('kv', 'tp'), scatter_dimension=1, tiled=...  28.9 us
    all_gather x1, blocking collectives, per_device(): full_rows = lax.all_gather(tokens, ('kv', 'tp'), axis=1, tiled=True)  16 us
    all_gather x1, blocking collectives, per_device(): gathered = lax.all_gather(branch, ('kv', 'tp'), axis=1, tiled=True)  14.1 us
    all_gather x1, blocking collectives, per_device(): whole_rows = lax.all_gather(residual_one, ('kv', 'tp'), axis=1, tiled=True)  14 us
    dot_general x1, matrix products, per_device(): partial_terms = jnp.dot(hidden, w_down, preferred_element_type=jnp.float32)  13.5 us
    all_to_all x1, waiting for transfers between devices, per_device(): lax.all_to_all(project(w_query), 'kv', split_axis=0, concat_axis=1, tiled...  5.57 us
    all_to_all x1, waiting for transfers between devices, per_device(): lax.all_to_all(project(w_input), 'kv', split_axis=0, concat_axis=1, tiled...  5.53 us
    all_to_all x1, waiting for transfers between devices, per_device(): lax.all_to_all(project(w_forget), 'kv', split_axis=0, concat_axis=1, tile...  5.41 us
  transfers between devices with their start and end apart: 5, of which 5 were waited for; matrix products, arithmetic and copies ran while one was open for 2% of the time, Pallas kernels for 0%

commit v1 on v0

--- a/solution.py
+++ b/solution.py
@@ -39,7 +39,12 @@
     query_raw, forget_raw, input_raw, gate_raw = (
         lax.all_to_all(project(w_query), "kv", split_axis=0, concat_axis=1, tiled=True),
         lax.all_to_all(project(w_forget), "kv", split_axis=0, concat_axis=1, tiled=True),
-        lax.all_to_all(project(w_input), "kv", split_axis=0, concat_axis=1, tiled=True),
+        jnp.concatenate(
+            lax.all_to_all(
+                jnp.stack(jnp.split(project(w_input), lax.axis_size("kv"), axis=0)), "kv", 0, 0
+            ),
+            axis=1,
+        ),
         lax.all_to_all(project(w_output_gate), "kv", split_axis=0, concat_axis=1, tiled=True),
     )
     seq_local = state.shape[0]

time: 147 us -> 147 us (level)
  transfers between devices with their start and end apart: 5 -> 5, of which waited for: 5 -> 5; matrix products, arithmetic and copies ran while one was open for 2% -> 3% of each run, Pallas kernels for 0% -> 0%
where the time goes in v1:
time: 147 us; the launch traced here: 146 us
  waiting for transfers between devices  45.9 us (31%)
  blocking collectives  44.1 us (30%)
  matrix products  19.9 us (14%)
  starting transfers between devices  15.7 us (11%)
  between operations  14.2 us (10%)
  other arithmetic  4.29 us (3%)
  local copies, waits for them, and re-layouts  2.2 us (1%)
    reduce_scatter x1, waiting for transfers between devices, per_device(): lax.psum_scatter(partial_terms, ('kv', 'tp'), scatter_dimension=1, tiled=...  28.9 us
    all_gather x1, blocking collectives, per_device(): full_rows = lax.all_gather(tokens, ('kv', 'tp'), axis=1, tiled=True)  16 us
    all_gather x1, blocking collectives, per_device(): gathered = lax.all_gather(branch, ('kv', 'tp'), axis=1, tiled=True)  14.1 us
    all_gather x1, blocking collectives, per_device(): whole_rows = lax.all_gather(residual_one, ('kv', 'tp'), axis=1, tiled=True)  14 us
    dot_general x1, matrix products, per_device(): partial_terms = jnp.dot(hidden, w_down, preferred_element_type=jnp.float32)  13.5 us
    all_to_all x1, waiting for transfers between devices, per_device(): lax.all_to_all(project(w_query), 'kv', split_axis=0, concat_axis=1, tiled...  5.57 us
    all_to_all x1, waiting for transfers between devices, per_device(): lax.all_to_all(jnp.stack(jnp.split(project(w_input), lax.axis_size('kv'),...  5.53 us
    all_to_all x1, waiting for transfers between devices, per_device(): lax.all_to_all(project(w_forget), 'kv', split_axis=0, concat_axis=1, tile...  5.41 us
  transfers between devices with their start and end apart: 5, of which 5 were waited for; matrix products, arithmetic and copies ran while one was open for 3% of the time, Pallas kernels for 0%

profile of v1, /device:TPU:0, one launch (start us, length us, event | category | flops | bytes accessed | tf_op | source)
XLA Modules:
  0.0 146.4 jit_solution(452440304205924939)
XLA Ops:
  7.2 0.0 copy-start
  7.2 0.0 copy-start.4
  7.2 0.0 copy-start.7
  7.2 16.0 %all_gather.9 = bf16[8,4096]{1,0:T(8,128)(2,1)S(1)} all-gather(bf16[8,512]{1,0:T(8,128)(2,1)} %param.13), channel_id=1, replica_groups=mesh['dp'=4,'kv'=4,'tp'=2] {'kv','tp'}, dimensions={1}, use_global_device_ids=true | all-gather | bytes 73728 | tf_op jit(solution)/shard_map/all_gather | solution.py:31
  23.2 0.1 fusion.24
  23.4 2.0 %fusion.20 = bf16[8,256]{1,0:T(8,128)(2,1)S(1)} fusion(bf16[4096,1,256]{2,0,1:T(8,128)(2,1)} %param.17, bf16[8,4096]{1,0:T(8,128)(2,1)S(1)} %all_gather.9, f32[4096]{0:T(1024)} %param.21, f32[8]{0:T(128)S(1)} %add_rsqrt_fusion.2), kind=kOutput, calls=%fused_computation.16 | convolution fusion | flops 16910336 | bytes 2183200 | tf_op jit(solution)/shard_map/dot_general | solution.py:35
  25.4 0.6 all_to_all.38
  26.0 4.6 %all-to-all-start.3 = ((bf16[4,2,256]{2,1,0:T(2,128)(2,1)}), bf16[4,2,256]{2,1,0:T(2,128)(2,1)S(1)}, u32[]{:S(2)}, u32[]{:S(2)}) async-start(bf16[4,2,256]{2,1,0:T(2,128)(2,1)} %all_to_all.38), calls=%async_computation.3 | async-start | bytes 8192 | tf_op jit(solution)/shard_map/all_to_all | solution.py:48
  30.7 0.0 copy-done.7
  30.7 0.0 copy-start.2
  30.7 0.0 copy-done.4
  30.7 0.0 copy-start.3
  30.7 2.2 %fusion.14 = bf16[8,256]{1,0:T(8,128)(2,1)S(1)} fusion(bf16[4096,1,256]{2,0,1:T(8,128)(2,1)} %param.15, bf16[8,4096]{1,0:T(8,128)(2,1)S(1)} %all_gather.9, f32[4096]{0:T(1024)S(1)} %copy-done.4, f32[8]{0:T(128)S(1)} %add_rsqrt_fusion.2), kind=kOutput, calls=%fused_computation.14 | convolution fusion | flops 16910336 | bytes 2183200 | tf_op jit(solution)/shard_map/dot_general | solution.py:35
  32.9 0.0 copy-done.2
  32.9 0.4 fusion.17
  33.3 0.2 copy-done.3
  33.5 0.4 fusion.11
  34.0 0.0 copy-start.8
  34.0 0.0 copy-start.5
  34.0 0.6 pad_maximum_fusion
  34.6 0.6 all_to_all.35
  35.2 0.6 all_to_all.33
  35.8 0.5 all-to-all-done.3
  36.3 4.6 %all-to-all-start = ((bf16[4,2,256]{2,1,0:T(2,128)(2,1)}), bf16[4,2,256]{2,1,0:T(2,128)(2,1)S(1)}, u32[]{:S(2)}, u32[]{:S(2)}) async-start(bf16[4,2,256]{2,1,0:T(2,128)(2,1)} %all_to_all.33), calls=%async_computation | async-start | bytes 8192 | tf_op jit(solution)/shard_map/all_to_all | solution.py:40
  40.9 5.6 %all-to-all-done = bf16[4,2,256]{2,1,0:T(2,128)(2,1)S(1)} async-done(((bf16[4,2,256]{2,1,0:T(2,128)(2,1)}), bf16[4,2,256]{2,1,0:T(2,128)(2,1)S(1)}, u32[]{:S(2)}, u32[]{:S(2)}) %all-to-all-start) | async-done | bytes 4128 | tf_op jit(solution)/shard_map/all_to_all | solution.py:40
  46.4 3.2 %all-to-all-start.2 = ((bf16[4,2,256]{2,1,0:T(2,128)(2,1)}), bf16[4,2,256]{2,1,0:T(2,128)(2,1)S(1)}, u32[]{:S(2)}, u32[]{:S(2)}) async-start(bf16[4,2,256]{2,1,0:T(2,128)(2,1)} %pad_maximum_fusion), calls=%async_computation.2 | async-start | bytes 8192 | tf_op jit(solution)/shard_map/all_to_all | solution.py:43
  49.7 5.5 %all-to-all-done.2 = bf16[4,2,256]{2,1,0:T(2,128)(2,1)S(1)} async-done(((bf16[4,2,256]{2,1,0:T(2,128)(2,1)}), bf16[4,2,256]{2,1,0:T(2,128)(2,1)S(1)}, u32[]{:S(2)}, u32[]{:S(2)}) %all-to-all-start.2) | async-done | bytes 4128 | tf_op jit(solution)/shard_map/all_to_all | solution.py:43
  55.2 3.2 %all-to-all-start.1 = ((bf16[4,2,256]{2,1,0:T(2,128)(2,1)}), bf16[4,2,256]{2,1,0:T(2,128)(2,1)S(1)}, u32[]{:S(2)}, u32[]{:S(2)}) async-start(bf16[4,2,256]{2,1,0:T(2,128)(2,1)} %all_to_all.35), calls=%async_computation.1 | async-start | bytes 8192 | tf_op jit(solution)/shard_map/all_to_all | solution.py:41
  58.4 0.0 reduce-scatter.2.cloned.1.call-start
  58.6 5.4 %all-to-all-done.1 = bf16[4,2,256]{2,1,0:T(2,128)(2,1)S(1)} async-done(((bf16[4,2,256]{2,1,0:T(2,128)(2,1)}), bf16[4,2,256]{2,1,0:T(2,128)(2,1)S(1)}, u32[]{:S(2)}, u32[]{:S(2)}) %all-to-all-start.1) | async-done | bytes 4128 | tf_op jit(solution)/shard_map/all_to_all | solution.py:41
  64.0 1.8 %multiply_add_fusion = f32[2,8,128,128]{3,2,1,0:T(8,128)S(1)} fusion(f32[2,8,128,128]{3,2,1,0:T(8,128)} %param.25, f32[2,8,128]{2,1,0:T(8,128)S(1)} %reshape.111, f32[2,8,128]{2,1,0:T(8,128)S(1)} %get-tuple-element.2, f32[2,8,128]{2,1,0:T(8,128)S(1)} %get-tuple-element.3), kind=kLoop, calls=%fused_computation.17 | loop fusion | flops 786432 | bytes 2121728 | tf_op jit(solution)/shard_map/add | solution.py:63
  65.9 0.0 copy-start.1
  65.9 0.0 copy-start.6
  65.9 1.0 fusion.42
  66.9 0.1 multiply_reduce_fusion
  67.0 0.0 copy-done.8
  67.0 0.1 multiply_convert_fusion
  67.1 14.1 %all_gather.10 = bf16[2,8,1024]{2,0,1:T(2,128)(2,1)S(1)} all-gather(bf16[2,1,1024]{2,0,1:T(2,128)(2,1)S(1)} %convert_element_type.111), channel_id=1, replica_groups=mesh['dp'=4,'kv'=4,'tp'=2] {'kv','tp'}, dimensions={1}, use_global_device_ids=true | all-gather | bytes 36864 | tf_op jit(solution)/shard_map/all_gather | solution.py:68
  81.2 0.0 copy-done
  81.2 0.0 copy-done.5
  81.2 0.4 fusion.10
  81.6 14.0 %all_gather.11 = bf16[8,4096]{1,0:T(8,128)(2,1)S(1)} all-gather(bf16[8,512]{1,0:T(8,128)(2,1)S(1)} %fusion.10), channel_id=1, replica_groups=mesh['dp'=4,'kv'=4,'tp'=2] {'kv','tp'}, dimensions={1}, use_global_device_ids=true | all-gather | bytes 73728 | tf_op jit(solution)/shard_map/all_gather | solution.py:75
  95.6 0.1 fusion.27
  95.7 0.0 copy-done.6
  95.8 13.5 %fusion.23 = f32[8,4096]{1,0:T(8,128)} fusion(bf16[2048,4096]{1,0:T(8,128)(2,1)} %param.24, bf16[4096,2048]{1,0:T(8,128)(2,1)} %param.23, bf16[8,4096]{1,0:T(8,128)(2,1)S(1)} %all_gather.11, f32[4096]{0:T(1024)S(1)} %copy-done.6, f32[8]{0:T(128)S(1)} %add_rsqrt_fusion.1), kind=kOutput, calls=%fused_computation.18 | convolution fusion | flops 268615680 | bytes 33767456 | tf_op jit(solution)/shard_map/dot_general | solution.py:79
  109.3 0.0 copy-done.1
  109.3 0.0 reduce-scatter.2.cloned.1.call-update
  109.3 28.9 %reduce-scatter.2.cloned.1.call-done = f32[8,512]{1,0:T(8,128)} async-done(((f32[8,4096]{1,0:T(8,128)}), f32[8,512]{1,0:T(8,128)}) %reduce-scatter.2.cloned.1.call-update) | async-done | bytes 16400 | tf_op jit(solution)/shard_map/reduce_scatter | solution.py:80
  138.2 1.3 add_convert_fusion
  (21 shorter events, 0.2 us)
Async XLA Ops:
  7.2 74.0 %copy-start = (bf16[2048,512]{1,0:T(8,128)(2,1)S(1)}, bf16[2048,512]{1,0:T(8,128)(2,1)}, u32[]{:S(2)}) copy-start(bf16[2048,512]{1,0:T(8,128)(2,1)} %param.20) | copy-start | bytes 6291460
  7.2 23.5 %copy-start.4 = (f32[4096]{0:T(1024)S(1)}, f32[4096]{0:T(1024)}, u32[]{:S(2)}) copy-start(f32[4096]{0:T(1024)} %param.21) | copy-start | bytes 49156
  7.2 23.5 %copy-start.7 = (f32[1024]{0:T(1024)S(1)}, f32[1024]{0:T(1024)}, u32[]{:S(2)}) copy-start(f32[1024]{0:T(1024)} %param.18) | copy-start | bytes 12292
  26.0 10.2 %all-to-all-start.3 = ((bf16[4,2,256]{2,1,0:T(2,128)(2,1)}), bf16[4,2,256]{2,1,0:T(2,128)(2,1)S(1)}, u32[]{:S(2)}, u32[]{:S(2)}) async-start(bf16[4,2,256]{2,1,0:T(2,128)(2,1)} %all_to_all.38), calls=%async_computation.3 | async-start | bytes 8192 | tf_op jit(solution)/shard_map/all_to_all | solution.py:48
  30.7 2.2 %copy-start.2 = (bf16[4096,1,256]{2,0,1:T(8,128)(2,1)S(1)}, bf16[4096,1,256]{2,0,1:T(8,128)(2,1)}, u32[]{:S(2)}) copy-start(bf16[4096,1,256]{2,0,1:T(8,128)(2,1)} %param.16) | copy-start | bytes 6291460
  30.7 2.8 %copy-start.3 = (bf16[4096,1,256]{2,0,1:T(8,128)(2,1)S(1)}, bf16[4096,1,256]{2,0,1:T(8,128)(2,1)}, u32[]{:S(2)}) copy-start(bf16[4096,1,256]{2,0,1:T(8,128)(2,1)} %param.14) | copy-start | bytes 6291460
  34.0 33.0 %copy-start.8 = (f32[128]{0:T(128)S(1)}, f32[128]{0:T(128)}, u32[]{:S(2)}) copy-start(f32[128]{0:T(128)} %param.19) | copy-start | bytes 1540
  34.0 47.3 %copy-start.5 = (bf16[8,512]{1,0:T(8,128)(2,1)S(1)}, bf16[8,512]{1,0:T(8,128)(2,1)}, u32[]{:S(2)}) copy-start(bf16[8,512]{1,0:T(8,128)(2,1)} %param.13) | copy-start | bytes 24580
  36.3 10.2 %all-to-all-start = ((bf16[4,2,256]{2,1,0:T(2,128)(2,1)}), bf16[4,2,256]{2,1,0:T(2,128)(2,1)S(1)}, u32[]{:S(2)}, u32[]{:S(2)}) async-start(bf16[4,2,256]{2,1,0:T(2,128)(2,1)} %all_to_all.33), calls=%async_computation | async-start | bytes 8192 | tf_op jit(solution)/shard_map/all_to_all | solution.py:40
  46.4 8.8 %all-to-all-start.2 = ((bf16[4,2,256]{2,1,0:T(2,128)(2,1)}), bf16[4,2,256]{2,1,0:T(2,128)(2,1)S(1)}, u32[]{:S(2)}, u32[]{:S(2)}) async-start(bf16[4,2,256]{2,1,0:T(2,128)(2,1)} %pad_maximum_fusion), calls=%async_computation.2 | async-start | bytes 8192 | tf_op jit(solution)/shard_map/all_to_all | solution.py:43
  55.2 8.8 %all-to-all-start.1 = ((bf16[4,2,256]{2,1,0:T(2,128)(2,1)}), bf16[4,2,256]{2,1,0:T(2,128)(2,1)S(1)}, u32[]{:S(2)}, u32[]{:S(2)}) async-start(bf16[4,2,256]{2,1,0:T(2,128)(2,1)} %all_to_all.35), calls=%async_computation.1 | async-start | bytes 8192 | tf_op jit(solution)/shard_map/all_to_all | solution.py:41
  58.4 79.8 %reduce-scatter.2.cloned.1.call-start = ((), (), s32[]{:S(2)}) async-start(), calls=%async_computation.5 | async-start | bytes 147456 | tf_op jit(solution)/shard_map/reduce_scatter | solution.py:80
  65.9 43.4 %copy-start.1 = (f32[2,8,128,128]{3,2,1,0:T(8,128)}, f32[2,8,128,128]{3,2,1,0:T(8,128)S(1)}, u32[]{:S(2)}) copy-start(f32[2,8,128,128]{3,2,1,0:T(8,128)S(1)} %multiply_add_fusion) | copy-start | bytes 3145732
  65.9 29.9 %copy-start.6 = (f32[4096]{0:T(1024)S(1)}, f32[4096]{0:T(1024)}, u32[]{:S(2)}) copy-start(f32[4096]{0:T(1024)} %param.22) | copy-start | bytes 49156
Sparse Core Ops, SparseCore 0:
  109.4 28.7 reduce-scatter.1
